TPU v7x, 32 devices: a whole 2x2x4 slice. The times are simulated.
32 devices in a mesh: grp: 2 (over y), sp: 4 (over z), tp: 4 (over x, core).
Axes of the slice: x: 2, y: 2, z: 4, core: 2. Of those that a mesh axis runs over, the one named last changes fastest.
Arguments:
- queries: bfloat16 [2048, 512], P(('grp', 'sp'), 'tp'), parts along dimension 0, may hold values from -6 to 6
- key_rows: bfloat16 [2048, 512], P(('grp', 'sp'), 'tp'), parts along dimension 0, may hold values from -6 to 6
- value_rows: bfloat16 [2048, 1024], P(('grp', 'sp'), 'tp'), parts along dimension 0, may hold values from -6 to 6
- out_gate: bfloat16 [2048, 1024], P(('grp', 'sp'), 'tp'), parts along dimension 0, may hold values from -6 to 6
- log_decay: float32 [2, 2048, 512], P(None, ('grp', 'sp'), 'tp'), parts along dimension 1
- doc_ids: int32 [2048], P(('grp', 'sp')), parts along dimension 0, may hold values from 0 to 1, as said below
- head_gain: float32 [1024], P('tp'), may hold values from 0.1 to 1.9
- out_weight: bfloat16 [1024, 2048], P('tp'), may hold values from -0.375 to 0.375
- residual: bfloat16 [2048, 2048], P(('grp', 'sp'), 'tp'), parts along dimension 0
- norm_gain: float32 [2, 2048], replicated, may hold values from 0.1 to 1.9
- norm_bias: float32 [2, 2048], replicated, may hold values from -3 to 3
- gate_weight: bfloat16 [2048, 3072], P('sp', 'tp'), may hold values from -0.125 to 0.125
- up_weight: bfloat16 [2048, 3072], P('sp', 'tp'), may hold values from -0.125 to 0.125
- down_weight: bfloat16 [3072, 2048], P('tp', 'sp'), may hold values from -0.109375 to 0.109375
Outputs:
- layer_out: bfloat16 [2048, 2048], P(('grp', 'sp'), 'tp'), parts along dimension 0
There are 2 independent parts, one for each index of `grp`. A program takes and returns all parts, laid end to end along the dimension named above; an argument that names none is the same for every part. Nothing has to cross between parts.
Inputs may be any that keep to these rules, and one draw needn't show every extreme that they name: `doc_ids`: document numbers start at 0 and never fall; they rise by one at each of 1 positions, the k-th rise lying within half of 256 positions of k times 1024 divided by 2.
All inputs are finite; a program needn't handle non-finite values.
Results may differ from a plain program's by a relative error of at most 0.009.
Values may be sent and summed in bfloat16 or wider, within the bound.
A program may use at most 128 MiB of HBM per device.

v0:
```python
import jax
import jax.numpy as jnp
from jax import lax
from jax.sharding import PartitionSpec as P

DK = 32
DV = 64
BLOCK = 64
EPS = 1e-06
HIGH = lax.Precision.HIGHEST


def entering(x, axis, combine, identity, reverse):
    peers, position = (lax.axis_size(axis), lax.axis_index(axis))
    everything = jax.tree.map(
        lambda part, kind: lax.all_gather(part.astype(kind), axis),
        x,
        jax.tree.map(lambda a: jnp.bfloat16 if a.dtype == jnp.float32 else a.dtype, x),
    )
    start = jax.tree.map(
        lambda part, zero: jnp.broadcast_to(jnp.asarray(zero, part.dtype), part.shape), x, identity
    )

    def hop(k, before):
        at = peers - 1 - k if reverse else k
        reached = at > position if reverse else at < position
        new = combine(
            before, jax.tree.map(lambda part, own: part[at].astype(own.dtype), everything, x)
        )
        return jax.tree.map(lambda a, b: jnp.where(reached, a, b), new, before)

    return lax.fori_loop(0, peers, hop, start)


def run_blocks(query, key_part, value_part, decay, docs):
    length = query.shape[0]
    count = length // BLOCK
    head_count = query.shape[1]
    lower = jnp.arange(BLOCK)[:, None] >= jnp.arange(BLOCK)[None, :]

    def blocked(array):
        return array.reshape((count, BLOCK) + array.shape[1:])

    def advance(carried, inputs):
        state, state_doc = carried
        query_block, key_block, value_block, decay_block, doc_block = inputs
        running = jnp.cumsum(decay_block, axis=0)
        allowed = lower & (doc_block[:, None] == doc_block[None, :])
        relative = jnp.exp(
            jnp.where(allowed[:, :, None, None], running[:, None] - running[None, :], -jnp.inf)
        )
        scores = jnp.einsum("ihd,jhd,ijhd->hij", query_block, key_block, relative, precision=HIGH)
        within = jnp.einsum("hij,jhe->ihe", scores, value_block, precision=HIGH)
        linked = (doc_block == state_doc).astype(jnp.float32)
        carried_part = (
            jnp.einsum("ihd,hde->ihe", query_block * jnp.exp(running), state, precision=HIGH)
            * linked[:, None, None]
        )
        closing = doc_block[-1]
        ending = (doc_block == closing).astype(jnp.float32)
        tail_decay = jnp.exp(running[-1][None] - running) * ending[:, None, None]
        kept = (state_doc == closing).astype(jnp.float32)
        state = kept * jnp.exp(running[-1])[:, :, None] * state + jnp.einsum(
            "jhd,jhe->hde", key_block * tail_decay, value_block, precision=HIGH
        )
        return ((state, closing), within + carried_part)

    start = (
        jnp.zeros((head_count, query.shape[2], value_part.shape[2]), jnp.float32),
        jnp.array(-1, jnp.int32),
    )
    (state, closing), outputs = lax.scan(
        advance,
        start,
        tuple((blocked(array) for array in (query, key_part, value_part, decay, docs))),
    )
    return (outputs.reshape(length, head_count, value_part.shape[2]), state, closing)


def chain(earlier, later):
    early_state, early_pass, early_entry, early_leave = earlier
    late_state, late_pass, late_entry, late_leave = later
    joined = (late_entry == early_leave) | (early_leave < 0.0) | (late_entry < 0.0)
    keep = jnp.where(joined, jnp.float32(1.0), jnp.float32(0.0))
    state = late_state + keep * late_pass[:, :, None] * early_state
    passing = keep * early_pass * late_pass
    entry = jnp.where(early_entry < 0.0, late_entry, early_entry)
    leaving = jnp.where(late_leave < 0.0, early_leave, late_leave)
    return (state, passing, entry, leaving)


def one_way(query, key_part, value_part, decay, docs, backward):
    local_out, state, closing = run_blocks(query, key_part, value_part, decay, docs)
    passing = jnp.exp(jnp.sum(decay, axis=0)) * (docs[0] == closing).astype(jnp.float32)
    piece = (state, passing, docs[0].astype(jnp.float32), closing.astype(jnp.float32))
    identity = (jnp.zeros_like(state), jnp.ones_like(passing), jnp.float32(-1.0), jnp.float32(-1.0))
    if backward:
        carried = entering(piece, "sp", chain, identity, True)
    else:
        carried = entering(piece, "sp", chain, identity, False)
    incoming, _, _, leaving = carried
    linked = (docs.astype(jnp.float32) == leaving).astype(jnp.float32)
    reach = query * jnp.exp(jnp.cumsum(decay, axis=0))
    return (
        local_out
        + jnp.einsum("ihd,hde->ihe", reach, incoming, precision=HIGH) * linked[:, None, None]
    )


def apply_norm(stream, moments, full_width, gain, bias):
    middle = moments[0][:, None] / full_width
    spread = moments[1][:, None] / full_width - middle * middle
    return (stream - middle) * lax.rsqrt(spread + EPS) * gain + bias


def on_device(
    queries,
    key_rows,
    value_rows,
    out_gate,
    log_decay,
    doc_ids,
    head_gain,
    out_weight,
    residual,
    norm_gain,
    norm_bias,
    gate_weight,
    up_weight,
    down_weight,
):
    collected = None
    length = queries.shape[0]
    head_count = queries.shape[1] // DK
    query = queries.astype(jnp.float32).reshape(length, head_count, DK) * DK ** (-0.5)
    key_part = key_rows.astype(jnp.float32).reshape(length, head_count, DK)
    value_part = value_rows.astype(jnp.float32).reshape(length, head_count, DV)
    forward_decay = log_decay[0].reshape(length, head_count, DK)
    backward_decay = log_decay[1].reshape(length, head_count, DK)
    forward_out = one_way(query, key_part, value_part, forward_decay, doc_ids, False)
    backward_out = one_way(
        query[::-1], key_part[::-1], value_part[::-1], backward_decay[::-1], doc_ids[::-1], True
    )[::-1]
    attended = forward_out + backward_out
    normed = attended * lax.rsqrt(jnp.mean(attended * attended, axis=-1, keepdims=True) + EPS)
    mixed = (
        normed.reshape(length, -1) * head_gain * jax.nn.silu(out_gate.astype(jnp.float32))
    ).astype(jnp.bfloat16)
    partial_value = jnp.dot(mixed, out_weight, preferred_element_type=jnp.float32)
    collected = (
        lax.all_gather(gate_weight, "sp", axis=0, tiled=True),
        lax.all_gather(up_weight, "sp", axis=0, tiled=True),
        lax.all_gather(down_weight, "sp", axis=1, tiled=True),
    )
    gate_full, up_full, down_full = collected
    own_width = residual.shape[1]
    full_width = own_width * lax.axis_size("tp")
    offset = lax.axis_index("tp") * own_width
    branch = lax.psum_scatter(
        partial_value.astype(jnp.bfloat16), "tp", scatter_dimension=1, tiled=True
    ).astype(jnp.float32)
    stream = residual.astype(jnp.float32) + branch
    moments = lax.psum((jnp.sum(stream, axis=1), jnp.sum(stream * stream, axis=1)), "tp")
    settled = apply_norm(
        stream,
        moments,
        full_width,
        lax.dynamic_slice_in_dim(norm_gain[0], offset, own_width, 0),
        lax.dynamic_slice_in_dim(norm_bias[0], offset, own_width, 0),
    )
    features = settled.astype(jnp.bfloat16)
    piece = lax.all_gather(features, "tp", axis=1, tiled=True)
    gate = jnp.dot(piece, gate_full, preferred_element_type=jnp.float32)
    up_part = jnp.dot(piece, up_full, preferred_element_type=jnp.float32)
    inner = (jax.nn.silu(gate) * up_part).astype(jnp.bfloat16)
    down = lax.psum_scatter(
        jnp.dot(inner, down_full, preferred_element_type=jnp.float32).astype(jnp.bfloat16),
        "tp",
        scatter_dimension=1,
        tiled=True,
    ).astype(jnp.float32)
    final = settled + 0.5 * down
    closing_moments = lax.psum((jnp.sum(final, axis=1), jnp.sum(final * final, axis=1)), "tp")
    result = apply_norm(
        final,
        closing_moments,
        full_width,
        lax.dynamic_slice_in_dim(norm_gain[1], offset, own_width, 0),
        lax.dynamic_slice_in_dim(norm_bias[1], offset, own_width, 0),
    )
    return result.astype(jnp.bfloat16)


def solution(mesh):
    in_specs = (
        P(("grp", "sp"), "tp"),
        P(("grp", "sp"), "tp"),
        P(("grp", "sp"), "tp"),
        P(("grp", "sp"), "tp"),
        P(None, ("grp", "sp"), "tp"),
        P(("grp", "sp")),
        P("tp"),
        P("tp", None),
        P(("grp", "sp"), "tp"),
        P(),
        P(),
        P("sp", "tp"),
        P("sp", "tp"),
        P("tp", "sp"),
    )
    out_specs = P(("grp", "sp"), "tp")
    return jax.shard_map(
        on_device, mesh=mesh, in_specs=in_specs, out_specs=out_specs, check_vma=False
    )
```

profile of v0, /device:TPU:0, one launch (start us, length us, event | category | flops | bytes accessed | tf_op | source)
XLA Modules:
  0.0 599.7 jit_solution(14972712356723388708)
XLA Ops:
  20.4 91.4 %while.66 = (s32[]{:T(128)}, f32[4,32,64]{2,1,0:T(8,128)S(1)}, s32[]{:T(128)}, f32[4,64,4,64]{1,0,3,2:T(4,128)}, s32[4,64]{1,0:T(4,128)S(1)}, /*index=5*/f32[4,6...) while((s32[]{:T(128)}, f32[4,32,64]{2,1,0:T(8,128)S(1)}, ...), condition=%wide.region_10.11_spmd.clone, body=%wide.region_8.10_spmd.clone.sunk | while | flops 28397956 | bytes 10073782 | solution.py:72
  24.7 5.8 copy.268
  37.0 4.5 dynamic_update_slice.12
  47.6 5.8 copy.268
  59.8 4.5 dynamic_update_slice.12
  70.5 5.8 copy.268
  82.7 4.5 dynamic_update_slice.12
  93.3 5.8 copy.268
  105.6 4.5 dynamic_update_slice.12
  117.5 88.7 %while.64 = (s32[]{:T(128)}, f32[4,32,64]{2,1,0:T(8,128)S(1)}, s32[]{:T(128)}, f32[4,64,4,64]{1,0,3,2:T(4,128)}, s32[4,64]{1,0:T(4,128)S(1)}, /*index=5*/f32[4,6...) while((s32[]{:T(128)}, f32[4,32,64]{2,1,0:T(8,128)S(1)}, ...), condition=%wide.region_2.3_spmd.clone, body=%wide.region_0.2_spmd.clone.sunk | while | flops 28397956 | bytes 10237110 | solution.py:72
  124.3 5.8 copy.262
  133.6 4.5 dynamic_update_slice.11
  146.5 5.8 copy.262
  155.8 4.5 dynamic_update_slice.11
  168.7 5.8 copy.262
  190.9 5.8 copy.262
  208.7 12.7 %all-gather.3 = bf16[4,4,32]{2,1,0:T(4,128)(2,1)S(1)} all-gather(bf16[1,4,32]{2,1,0:T(4,128)(2,1)S(1)} %fusion.57), channel_id=4, replica_groups=mesh['grp'=2,'sp'=4,'tp'=4] {'sp'}, dimensions={0}, use_global_device_ids=true | all-gather | bytes 1280 | tf_op jit(solution)/shard_map/all_gather | solution.py:16
  221.4 13.4 %all-gather.1 = bf16[16,32,64]{2,1,0:T(8,128)(2,1)S(1)} all-gather(bf16[4,32,64]{2,1,0:T(8,128)(2,1)S(1)} %convert_element_type.257), channel_id=3, replica_groups=mesh['grp'=2,'sp'=4,'tp'=4] {'sp'}, dimensions={0}, use_global_device_ids=true | all-gather | bytes 81920 | tf_op jit(solution)/shard_map/all_gather | solution.py:16
  238.4 8.5 %all-reduce.6 = (bf16[4]{0:T(256)(128)(2,1)S(1)}, bf16[4]{0:T(256)(128)(2,1)S(1)}, bf16[4]{0:T(256)(128)(2,1)S(1)}, bf16[4]{0:T(256)(128)(2,1)S(1)}) all-reduce(bf16[4]{0:T(256)(128)(2,1)S(1)} %dynamic-update-slice.2, bf16[4]{0:T(256)(128)(2,1)S(1)} %dynamic-update-slice.3, ...), channel_id=1, replica_groups=mesh['grp'=2,'sp'=4,'tp'=4] {'sp'}, use_global_device_ids=true, to_apply=%add.2 | all-reduce | flops 16 | bytes 64
  246.9 15.9 %while.67 = (s32[]{:T(128)}, f32[4,32,64]{2,1,0:T(8,128)S(1)}, f32[]{:T(128)}, s32[]{:T(128)}, bf16[4,4,32,64]{3,2,1,0:T(8,128)(2,1)S(1)}, /*index=5*/bf16[4]{0:...) while((s32[]{:T(128)}, f32[4,32,64]{2,1,0:T(8,128)S(1)}, ...), condition=%wide.region_13.14_spmd.clone, body=%wide.region_12.13_spmd.clone.sunk | while | flops 41233 | bytes 83500 | solution.py:32
  269.5 9.6 %all_gather.60 = bf16[4,4,32]{2,1,0:T(4,128)(2,1)S(1)} all-gather(bf16[1,4,32]{2,1,0:T(4,128)(2,1)S(1)} %convert_element_type.252), channel_id=1, replica_groups=mesh['grp'=2,'sp'=4,'tp'=4] {'sp'}, dimensions={0}, use_global_device_ids=true | all-gather | bytes 1280 | tf_op jit(solution)/shard_map/all_gather | solution.py:16
  279.1 13.4 %all-gather = bf16[16,32,64]{2,1,0:T(8,128)(2,1)S(1)} all-gather(bf16[4,32,64]{2,1,0:T(8,128)(2,1)S(1)} %convert_element_type.247), channel_id=2, replica_groups=mesh['grp'=2,'sp'=4,'tp'=4] {'sp'}, dimensions={0}, use_global_device_ids=true | all-gather | bytes 81920 | tf_op jit(solution)/shard_map/all_gather | solution.py:16
  292.5 15.8 %while.65 = (s32[]{:T(128)}, f32[4,32,64]{2,1,0:T(8,128)S(1)}, f32[]{:T(128)}, s32[]{:T(128)}, bf16[4,4,32,64]{3,2,1,0:T(8,128)(2,1)S(1)}, /*index=5*/bf16[4]{0:...) while((s32[]{:T(128)}, f32[4,32,64]{2,1,0:T(8,128)S(1)}, ...), condition=%wide.region_5.6_spmd.clone, body=%wide.region_4.5_spmd.clone.sunk | while | flops 41229 | bytes 83438 | solution.py:32
  313.6 23.0 %reduce-scatter.3.cloned.1.call-done = bf16[256,512]{1,0:T(8,128)(2,1)} async-done(((bf16[256,2048]{1,0:T(8,128)(2,1)}), bf16[256,512]{1,0:T(8,128)(2,1)}) %reduce-scatter.3.cloned.1.call-update) | async-done | bytes 262160 | tf_op jit(solution)/shard_map/reduce_scatter | solution.py:159
  337.8 5.8 all-reduce.5
  347.4 15.5 %all-gather.9.cloned.1.call-done = bf16[256,2048]{1,0:T(8,128)(2,1)} async-done(((bf16[256,512]{1,0:T(8,128)(2,1)}), bf16[256,2048]{1,0:T(8,128)(2,1)}) %all-gather.9.cloned.1.call-update) | async-done | bytes 1048592 | tf_op jit(solution)/shard_map/all_gather | solution.py:172
  362.9 65.1 %all-gather.11.cloned.1.call-done = bf16[2048,768]{1,0:T(8,128)(2,1)} async-done(((bf16[512,768]{1,0:T(8,128)(2,1)}), bf16[2048,768]{1,0:T(8,128)(2,1)}) %all-gather.11.cloned.1.call-update) | async-done | bytes 3145744 | tf_op jit(solution)/shard_map/all_gather | solution.py:151
  432.1 59.5 %all-gather.13.cloned.1.call-done = bf16[2048,768]{1,0:T(8,128)(2,1)} async-done(((bf16[512,768]{1,0:T(8,128)(2,1)}), bf16[2048,768]{1,0:T(8,128)(2,1)}) %all-gather.13.cloned.1.call-update) | async-done | bytes 3145744 | tf_op jit(solution)/shard_map/all_gather | solution.py:152
  491.5 63.5 %all-gather.15.cloned.1.call-done = bf16[768,2048]{1,0:T(8,128)(2,1)} async-done(((bf16[768,512]{1,0:T(8,128)(2,1)}), bf16[768,2048]{1,0:T(8,128)(2,1)}) %all-gather.15.cloned.1.call-update) | async-done | bytes 3145744 | tf_op jit(solution)/shard_map/all_gather | solution.py:153
  555.1 6.2 %convolution_convert_fusion.1 = bf16[256,2048]{1,0:T(8,128)(2,1)} fusion(bf16[768,2048]{1,0:T(8,128)(2,1)} %all-gather.15.cloned.1.call-done, bf16[256,2048]{1,0:T(8,128)(2,1)S(1)} %copy-done.14, bf16[2048,768]{1,0:T(8,128)(2,1)} %all-gather.13.cloned.1.call-done, f32[256,768]{1,0:T(8,128)} %fusion.68), kind=kOutput, calls=%fused_computation.68 | convolution fusion | flops 1612316672 | bytes 9175040 | tf_op jit(solution)/shard_map/dot_general | solution.py:177
  561.3 23.6 %reduce-scatter.5.cloned.1.call-done = bf16[256,512]{1,0:T(8,128)(2,1)} async-done(((bf16[256,2048]{1,0:T(8,128)(2,1)}), bf16[256,512]{1,0:T(8,128)(2,1)}) %reduce-scatter.5.cloned.1.call-update) | async-done | bytes 262160 | tf_op jit(solution)/shard_map/reduce_scatter | solution.py:176
  586.2 5.8 all-reduce.4
  (321 shorter events, 151.8 us)
Async XLA Ops:
  6.5 305.4 %copy-start = (bf16[256,2048]{1,0:T(8,128)(2,1)S(1)}, bf16[256,2048]{1,0:T(8,128)(2,1)}, u32[]{:S(2)}) copy-start(bf16[256,2048]{1,0:T(8,128)(2,1)} %param.29) | copy-start | bytes 3145732
  6.5 330.2 %reduce-scatter.3.cloned.1.call-start = ((), (), s32[]{:S(2)}) async-start(), calls=%async_computation.2 | async-start | bytes 1310720 | tf_op jit(solution)/shard_map/reduce_scatter | solution.py:159
  14.6 98.4 %copy-start.5 = (f32[256,4,32]{0,2,1:T(8,128)}, f32[256,4,32]{0,2,1:T(8,128)S(1)}, u32[]{:S(2)}) copy-start(f32[256,4,32]{0,2,1:T(8,128)S(1)} %rev.19) | copy-start | bytes 393220
  16.6 3.8 copy-start.9
  17.4 3.0 copy-start.8
  114.7 2.9 copy-start.6
  117.5 117.2 %copy-start.17 = (u32[32]{0:T(128)S(1)}, u32[32]{0:T(128)}, u32[]{:S(2)}) copy-start(u32[32]{0:T(128)} %constant.182) | copy-start | bytes 388
  117.5 145.3 %copy-start.3 = (f32[4,64,4,64]{1,0,3,2:T(4,128)S(1)}, f32[4,64,4,64]{1,0,3,2:T(4,128)}, u32[]{:S(2)}) copy-start(f32[4,64,4,64]{1,0,3,2:T(4,128)} %get-tuple-element.457) | copy-start | bytes 786436
  206.3 102.0 %copy-start.11 = (s32[256]{0:T(256)S(1)}, s32[256]{0:T(256)}, u32[]{:S(2)}) copy-start(s32[256]{0:T(256)} %param.27) | copy-start | bytes 3076
  206.3 102.0 %copy-start.4 = (f32[4,64,4,64]{1,0,3,2:T(4,128)S(1)}, f32[4,64,4,64]{1,0,3,2:T(4,128)}, u32[]{:S(2)}) copy-start(f32[4,64,4,64]{1,0,3,2:T(4,128)} %get-tuple-element.452) | copy-start | bytes 786436
  206.3 102.4 %copy-start.7 = (f32[1,256,128]{1,2,0:T(8,128)S(1)}, f32[1,256,128]{1,2,0:T(8,128)}, u32[]{:S(2)}) copy-start(f32[1,256,128]{1,2,0:T(8,128)} %copy-done.6) | copy-start | bytes 393220
  206.3 104.9 %copy-start.10 = (bf16[256,128]{0,1:T(8,128)(2,1)S(1)}, bf16[256,128]{0,1:T(8,128)(2,1)}, u32[]{:S(2)}) copy-start(bf16[256,128]{0,1:T(8,128)(2,1)} %copy-done.9) | copy-start | bytes 196612
  246.9 65.1 %copy-start.15 = (bf16[256,256]{1,0:T(8,128)(2,1)S(1)}, bf16[256,256]{1,0:T(8,128)(2,1)}, u32[]{:S(2)}) copy-start(bf16[256,256]{1,0:T(8,128)(2,1)} %param.25) | copy-start | bytes 393220
  246.9 65.1 %copy-start.16 = (f32[256]{0:T(256)S(1)}, f32[256]{0:T(256)}, u32[]{:S(2)}) copy-start(f32[256]{0:T(256)} %param.28) | copy-start | bytes 3076
  292.5 21.1 %copy-start.12 = (f32[2,2048]{1,0:T(2,128)S(1)}, f32[2,2048]{1,0:T(2,128)}, u32[]{:S(2)}) copy-start(f32[2,2048]{1,0:T(2,128)} %param.31) | copy-start | bytes 49156
  292.5 21.1 %copy-start.13 = (f32[2,2048]{1,0:T(2,128)S(1)}, f32[2,2048]{1,0:T(2,128)}, u32[]{:S(2)}) copy-start(f32[2,2048]{1,0:T(2,128)} %param.32) | copy-start | bytes 49156
  292.5 44.2 %copy-start.1 = (bf16[256,512]{1,0:T(8,128)(2,1)S(1)}, bf16[256,512]{1,0:T(8,128)(2,1)}, u32[]{:S(2)}) copy-start(bf16[256,512]{1,0:T(8,128)(2,1)} %param.30) | copy-start | bytes 786436
  313.5 49.4 %all-gather.9.cloned.1.call-start = ((), (), s32[]{:S(2)}) async-start(), calls=%async_computation.3 | async-start | bytes 1310720 | tf_op jit(solution)/shard_map/all_gather | solution.py:172
  345.5 82.5 %all-gather.11.cloned.1.call-start = ((), (), s32[]{:S(2)}) async-start(), calls=%async_computation.4 | async-start | bytes 3932160 | tf_op jit(solution)/shard_map/all_gather | solution.py:151
  346.2 145.3 %all-gather.13.cloned.1.call-start = ((), (), s32[]{:S(2)}) async-start(), calls=%async_computation.5 | async-start | bytes 3932160 | tf_op jit(solution)/shard_map/all_gather | solution.py:152
  346.8 208.3 %all-gather.15.cloned.1.call-start = ((), (), s32[]{:S(2)}) async-start(), calls=%async_computation.6 | async-start | bytes 3932160 | tf_op jit(solution)/shard_map/all_gather | solution.py:153
  347.4 237.5 %reduce-scatter.5.cloned.1.call-start = ((), (), s32[]{:S(2)}) async-start(), calls=%async_computation.7 | async-start | bytes 1310720 | tf_op jit(solution)/shard_map/reduce_scatter | solution.py:176
  362.9 192.1 %copy-start.14 = (bf16[256,2048]{1,0:T(8,128)(2,1)S(1)}, bf16[256,2048]{1,0:T(8,128)(2,1)}, u32[]{:S(2)}) copy-start(bf16[256,2048]{1,0:T(8,128)(2,1)} %all-gather.9.cloned.1.call-done) | copy-start | bytes 3145732
  432.1 152.8 %copy-start.2 = (bf16[256,512]{1,0:T(8,128)(2,1)S(1)}, bf16[256,512]{1,0:T(8,128)(2,1)}, u32[]{:S(2)}) copy-start(bf16[256,512]{1,0:T(8,128)(2,1)} %reduce-scatter.3.cloned.1.call-done) | copy-start | bytes 786436
Sparse Core Ops, SparseCore 0:
  313.6 23.0 reduce-scatter.2
  345.6 17.3 all-gather.8
  364.5 63.4 all-gather.10
  429.4 62.0 all-gather.12
  492.9 62.0 all-gather.14
  561.4 23.4 reduce-scatter.4
where the time goes:
time: 603 us; the launch traced here: 600 us
  waiting for transfers between devices  252 us (42%)
  local copies, waits for them, and re-layouts  132 us (22%)
  other arithmetic  75.6 us (13%)
  blocking collectives  69.1 us (11%)
  loops' own time  32.7 us (5%)
  matrix products  22 us (4%)
  between operations  16.4 us (3%)
    all_gather x1, waiting for transfers between devices, on_device(): lax.all_gather(gate_weight, 'sp', axis=0, tiled=True)  65.1 us
    all_gather x1, waiting for transfers between devices, on_device(): lax.all_gather(down_weight, 'sp', axis=1, tiled=True)  63.5 us
    all_gather x1, waiting for transfers between devices, on_device(): lax.all_gather(up_weight, 'sp', axis=0, tiled=True)  59.5 us
    all_gather x4, blocking collectives, entering(): lax.all_gather(part.astype(kind), axis)  49 us
    while x8, local copies, waits for them, and re-layouts  46.3 us
    dynamic_update_slice x8, local copies, waits for them, and re-layouts, run_blocks(): lax.scan(advance, start, tuple((blocked(array) for array in (query, key_p...  35.8 us
    while x8, other arithmetic  25.3 us
    reduce_scatter x1, waiting for transfers between devices, on_device(): lax.psum_scatter(jnp.dot(inner, down_full, preferred_element_type=jnp.flo...  23.6 us
  transfers between devices with their start and end apart: 6, of which 6 were waited for; matrix products, arithmetic and copies ran while one was open for 1% of the time, Pallas kernels for 0%

commit v1 on v0

--- a/solution.py
+++ b/solution.py
@@ -150,7 +150,7 @@
     collected = (
         lax.all_gather(gate_weight, "sp", axis=0, tiled=True),
         lax.all_gather(up_weight, "sp", axis=0, tiled=True),
-        lax.all_gather(down_weight, "sp", axis=1, tiled=True),
+        jnp.concatenate(lax.all_gather(down_weight, "sp"), axis=1),
     )
     gate_full, up_full, down_full = collected
     own_width = residual.shape[1]

time: 603 us -> 571 us (0.947)
  waiting for transfers between devices: 252 us -> 214 us
    all_gather x1, waiting for transfers between devices: 63.5 us -> 30 us  [on_device(): lax.all_gather(down_weight, 'sp')]
  transfers between devices with their start and end apart: 6 -> 6, of which waited for: 6 -> 6; matrix products, arithmetic and copies ran while one was open for 1% -> 2% of each run, Pallas kernels for 0% -> 0%
where the time goes in v1:
time: 571 us; the launch traced here: 568 us
  waiting for transfers between devices  214 us (37%)
  local copies, waits for them, and re-layouts  136 us (24%)
  other arithmetic  75.6 us (13%)
  blocking collectives  69.4 us (12%)
  loops' own time  32.7 us (6%)
  matrix products  22 us (4%)
  between operations  18.1 us (3%)
    all_gather x1, waiting for transfers between devices, on_device(): lax.all_gather(gate_weight, 'sp', axis=0, tiled=True)  64.8 us
    all_gather x1, waiting for transfers between devices, on_device(): lax.all_gather(up_weight, 'sp', axis=0, tiled=True)  59.5 us
    all_gather x4, blocking collectives, entering(): lax.all_gather(part.astype(kind), axis)  49 us
    while x8, local copies, waits for them, and re-layouts  46.3 us
    dynamic_update_slice x8, local copies, waits for them, and re-layouts, run_blocks(): lax.scan(advance, start, tuple((blocked(array) for array in (query, key_p...  35.8 us
    all_gather x1, waiting for transfers between devices, on_device(): lax.all_gather(down_weight, 'sp')  30 us
    while x8, other arithmetic  25.3 us
    reduce_scatter x1, waiting for transfers between devices, on_device(): lax.psum_scatter(jnp.dot(inner, down_full, preferred_element_type=jnp.flo...  23.6 us
  transfers between devices with their start and end apart: 6, of which 6 were waited for; matrix products, arithmetic and copies ran while one was open for 2% of the time, Pallas kernels for 0%

profile of v1, /device:TPU:0, one launch (start us, length us, event | category | flops | bytes accessed | tf_op | source)
XLA Modules:
  0.0 568.4 jit_solution(12712363311007943028)
XLA Ops:
  21.2 91.4 %while.66 = (s32[]{:T(128)}, f32[4,32,64]{2,1,0:T(8,128)S(1)}, s32[]{:T(128)}, f32[4,64,4,64]{1,0,3,2:T(4,128)}, s32[4,64]{1,0:T(4,128)S(1)}, /*index=5*/f32[4,6...) while((s32[]{:T(128)}, f32[4,32,64]{2,1,0:T(8,128)S(1)}, ...), condition=%wide.region_10.11_spmd.clone, body=%wide.region_8.10_spmd.clone.sunk | while | flops 28397956 | bytes 10073782 | solution.py:72
  25.6 5.8 %copy.305 = f32[4,64,64,32]{1,2,3,0:T(8,128)} copy(f32[4,64,64,32]{2,3,0,1:T(8,128)} %exponential_bitcast_fusion.11) | data formatting | bytes 4194304 | tf_op jit(solution)/shard_map/while
  37.8 4.5 dynamic_update_slice.12
  48.4 5.8 %copy.305 = f32[4,64,64,32]{1,2,3,0:T(8,128)} copy(f32[4,64,64,32]{2,3,0,1:T(8,128)} %exponential_bitcast_fusion.11) | data formatting | bytes 4194304 | tf_op jit(solution)/shard_map/while
  60.7 4.5 dynamic_update_slice.12
  71.3 5.8 %copy.305 = f32[4,64,64,32]{1,2,3,0:T(8,128)} copy(f32[4,64,64,32]{2,3,0,1:T(8,128)} %exponential_bitcast_fusion.11) | data formatting | bytes 4194304 | tf_op jit(solution)/shard_map/while
  83.5 4.5 dynamic_update_slice.12
  94.2 5.8 %copy.305 = f32[4,64,64,32]{1,2,3,0:T(8,128)} copy(f32[4,64,64,32]{2,3,0,1:T(8,128)} %exponential_bitcast_fusion.11) | data formatting | bytes 4194304 | tf_op jit(solution)/shard_map/while
  106.4 4.5 dynamic_update_slice.12
  118.4 88.7 %while.64 = (s32[]{:T(128)}, f32[4,32,64]{2,1,0:T(8,128)S(1)}, s32[]{:T(128)}, f32[4,64,4,64]{1,0,3,2:T(4,128)}, s32[4,64]{1,0:T(4,128)S(1)}, /*index=5*/f32[4,6...) while((s32[]{:T(128)}, f32[4,32,64]{2,1,0:T(8,128)S(1)}, ...), condition=%wide.region_2.3_spmd.clone, body=%wide.region_0.2_spmd.clone.sunk | while | flops 28397956 | bytes 10237110 | solution.py:72
  125.2 5.8 %copy.299 = f32[4,64,64,32]{1,2,3,0:T(8,128)} copy(f32[4,64,64,32]{2,3,0,1:T(8,128)} %exponential_bitcast_fusion.10) | data formatting | bytes 4194304 | tf_op jit(solution)/shard_map/while
  134.4 4.5 dynamic_update_slice.11
  147.4 5.8 %copy.299 = f32[4,64,64,32]{1,2,3,0:T(8,128)} copy(f32[4,64,64,32]{2,3,0,1:T(8,128)} %exponential_bitcast_fusion.10) | data formatting | bytes 4194304 | tf_op jit(solution)/shard_map/while
  169.5 5.8 %copy.299 = f32[4,64,64,32]{1,2,3,0:T(8,128)} copy(f32[4,64,64,32]{2,3,0,1:T(8,128)} %exponential_bitcast_fusion.10) | data formatting | bytes 4194304 | tf_op jit(solution)/shard_map/while
  191.7 5.8 %copy.299 = f32[4,64,64,32]{1,2,3,0:T(8,128)} copy(f32[4,64,64,32]{2,3,0,1:T(8,128)} %exponential_bitcast_fusion.10) | data formatting | bytes 4194304 | tf_op jit(solution)/shard_map/while
  209.5 12.7 %all-gather.4 = bf16[4,4,32]{2,1,0:T(4,128)(2,1)S(1)} all-gather(bf16[1,4,32]{2,1,0:T(4,128)(2,1)S(1)} %fusion.57), channel_id=4, replica_groups=mesh['grp'=2,'sp'=4,'tp'=4] {'sp'}, dimensions={0}, use_global_device_ids=true | all-gather | bytes 1280 | tf_op jit(solution)/shard_map/all_gather | solution.py:16
  222.2 13.4 %all-gather.1 = bf16[16,32,64]{2,1,0:T(8,128)(2,1)S(1)} all-gather(bf16[4,32,64]{2,1,0:T(8,128)(2,1)S(1)} %convert_element_type.257), channel_id=3, replica_groups=mesh['grp'=2,'sp'=4,'tp'=4] {'sp'}, dimensions={0}, use_global_device_ids=true | all-gather | bytes 81920 | tf_op jit(solution)/shard_map/all_gather | solution.py:16
  239.2 8.5 %all-reduce.6 = (bf16[4]{0:T(256)(128)(2,1)S(1)}, bf16[4]{0:T(256)(128)(2,1)S(1)}, bf16[4]{0:T(256)(128)(2,1)S(1)}, bf16[4]{0:T(256)(128)(2,1)S(1)}) all-reduce(bf16[4]{0:T(256)(128)(2,1)S(1)} %dynamic-update-slice.2, bf16[4]{0:T(256)(128)(2,1)S(1)} %dynamic-update-slice.3, ...), channel_id=1, replica_groups=mesh['grp'=2,'sp'=4,'tp'=4] {'sp'}, use_global_device_ids=true, to_apply=%add.2 | all-reduce | flops 16 | bytes 64
  247.7 15.9 %while.67 = (s32[]{:T(128)}, f32[4,32,64]{2,1,0:T(8,128)S(1)}, f32[]{:T(128)}, s32[]{:T(128)}, bf16[4,4,32,64]{3,2,1,0:T(8,128)(2,1)S(1)}, /*index=5*/bf16[4]{0:...) while((s32[]{:T(128)}, f32[4,32,64]{2,1,0:T(8,128)S(1)}, ...), condition=%wide.region_13.14_spmd.clone, body=%wide.region_12.13_spmd.clone.sunk | while | flops 41233 | bytes 83500 | solution.py:32
  270.3 9.6 %all_gather.63 = bf16[4,4,32]{2,1,0:T(4,128)(2,1)S(1)} all-gather(bf16[1,4,32]{2,1,0:T(4,128)(2,1)S(1)} %convert_element_type.252), channel_id=1, replica_groups=mesh['grp'=2,'sp'=4,'tp'=4] {'sp'}, dimensions={0}, use_global_device_ids=true | all-gather | bytes 1280 | tf_op jit(solution)/shard_map/all_gather | solution.py:16
  279.9 13.4 %all-gather = bf16[16,32,64]{2,1,0:T(8,128)(2,1)S(1)} all-gather(bf16[4,32,64]{2,1,0:T(8,128)(2,1)S(1)} %convert_element_type.247), channel_id=2, replica_groups=mesh['grp'=2,'sp'=4,'tp'=4] {'sp'}, dimensions={0}, use_global_device_ids=true | all-gather | bytes 81920 | tf_op jit(solution)/shard_map/all_gather | solution.py:16
  293.3 15.8 %while.65 = (s32[]{:T(128)}, f32[4,32,64]{2,1,0:T(8,128)S(1)}, f32[]{:T(128)}, s32[]{:T(128)}, bf16[4,4,32,64]{3,2,1,0:T(8,128)(2,1)S(1)}, /*index=5*/bf16[4]{0:...) while((s32[]{:T(128)}, f32[4,32,64]{2,1,0:T(8,128)S(1)}, ...), condition=%wide.region_5.6_spmd.clone, body=%wide.region_4.5_spmd.clone.sunk | while | flops 41229 | bytes 83438 | solution.py:32
  315.1 22.5 %reduce-scatter.3.cloned.1.call-done = bf16[256,512]{1,0:T(8,128)(2,1)} async-done(((bf16[256,2048]{1,0:T(8,128)(2,1)}), bf16[256,512]{1,0:T(8,128)(2,1)}) %reduce-scatter.3.cloned.1.call-update) | async-done | bytes 262160 | tf_op jit(solution)/shard_map/reduce_scatter | solution.py:159
  338.7 6.1 %all-reduce.5 = (f32[256]{0:T(256)S(1)}, f32[256]{0:T(256)S(1)}) all-reduce(f32[256]{0:T(256)S(1)} %get-tuple-element.673, f32[256]{0:T(256)S(1)} %get-tuple-element.672), channel_id=1, replica_groups=mesh['grp'=2,'sp'=4,'tp'=4] {'tp'}, use_global_device_ids=true, to_apply=%region_21.22 | all-reduce | flops 512 | bytes 4096 | tf_op jit(solution)/shard_map/psum | solution.py:163
  348.0 30.0 %all-gather.16.cloned.1.call-done = bf16[3072,512]{1,0:T(8,128)(2,1)} async-done(((bf16[768,512]{1,0:T(8,128)(2,1)}), bf16[3072,512]{1,0:T(8,128)(2,1)}) %all-gather.16.cloned.1.call-update) | async-done | bytes 3145744 | tf_op jit(solution)/shard_map/all_gather | solution.py:153
  378.0 4.7 copy.204
  382.7 12.0 %all-gather.10.cloned.1.call-done = bf16[256,2048]{1,0:T(8,128)(2,1)} async-done(((bf16[256,512]{1,0:T(8,128)(2,1)}), bf16[256,2048]{1,0:T(8,128)(2,1)}) %all-gather.10.cloned.1.call-update) | async-done | bytes 1048592 | tf_op jit(solution)/shard_map/all_gather | solution.py:172
  394.7 64.8 %all-gather.12.cloned.1.call-done = bf16[2048,768]{1,0:T(8,128)(2,1)} async-done(((bf16[512,768]{1,0:T(8,128)(2,1)}), bf16[2048,768]{1,0:T(8,128)(2,1)}) %all-gather.12.cloned.1.call-update) | async-done | bytes 3145744 | tf_op jit(solution)/shard_map/all_gather | solution.py:151
  463.5 59.5 %all-gather.14.cloned.1.call-done = bf16[2048,768]{1,0:T(8,128)(2,1)} async-done(((bf16[512,768]{1,0:T(8,128)(2,1)}), bf16[2048,768]{1,0:T(8,128)(2,1)}) %all-gather.14.cloned.1.call-update) | async-done | bytes 3145744 | tf_op jit(solution)/shard_map/all_gather | solution.py:152
  523.0 6.3 %convolution_convert_fusion.1 = bf16[256,2048]{1,0:T(8,128)(2,1)} fusion(bf16[768,2048]{0,1:T(8,128)(2,1)} %bitcast.312, bf16[256,2048]{1,0:T(8,128)(2,1)S(1)} %copy-done.14, bf16[2048,768]{1,0:T(8,128)(2,1)} %all-gather.14.cloned.1.call-done, f32[256,768]{1,0:T(8,128)} %fusion.68), kind=kOutput, calls=%fused_computation.68 | convolution fusion | flops 1612316672 | bytes 9175040 | tf_op jit(solution)/shard_map/dot_general | solution.py:177
  529.3 23.6 %reduce-scatter.5.cloned.1.call-done = bf16[256,512]{1,0:T(8,128)(2,1)} async-done(((bf16[256,2048]{1,0:T(8,128)(2,1)}), bf16[256,512]{1,0:T(8,128)(2,1)}) %reduce-scatter.5.cloned.1.call-update) | async-done | bytes 262160 | tf_op jit(solution)/shard_map/reduce_scatter | solution.py:176
  554.2 5.8 %all-reduce.4 = (f32[256]{0:T(256)S(1)}, f32[256]{0:T(256)S(1)}) all-reduce(f32[256]{0:T(256)S(1)} %get-tuple-element.671, f32[256]{0:T(256)S(1)} %get-tuple-element.670), channel_id=1, replica_groups=mesh['grp'=2,'sp'=4,'tp'=4] {'tp'}, use_global_device_ids=true, to_apply=%region_26.27 | all-reduce | flops 512 | bytes 4096 | tf_op jit(solution)/shard_map/psum | solution.py:183
  (322 shorter events, 156.3 us)
Async XLA Ops:
  7.4 305.5 %copy-start = (bf16[256,2048]{1,0:T(8,128)(2,1)S(1)}, bf16[256,2048]{1,0:T(8,128)(2,1)}, u32[]{:S(2)}) copy-start(bf16[256,2048]{1,0:T(8,128)(2,1)} %param.29) | copy-start | bytes 3145732
  7.4 330.2 %reduce-scatter.3.cloned.1.call-start = ((), (), s32[]{:S(2)}) async-start(), calls=%async_computation.2 | async-start | bytes 1310720 | tf_op jit(solution)/shard_map/reduce_scatter | solution.py:159
  15.4 98.4 %copy-start.5 = (f32[256,4,32]{0,2,1:T(8,128)}, f32[256,4,32]{0,2,1:T(8,128)S(1)}, u32[]{:S(2)}) copy-start(f32[256,4,32]{0,2,1:T(8,128)S(1)} %rev.19) | copy-start | bytes 393220
  17.4 3.8 copy-start.9
  18.2 3.0 copy-start.8
  115.5 2.9 copy-start.6
  118.4 117.2 %copy-start.17 = (u32[32]{0:T(128)S(1)}, u32[32]{0:T(128)}, u32[]{:S(2)}) copy-start(u32[32]{0:T(128)} %constant.182) | copy-start | bytes 388
  118.4 145.3 %copy-start.3 = (f32[4,64,4,64]{1,0,3,2:T(4,128)S(1)}, f32[4,64,4,64]{1,0,3,2:T(4,128)}, u32[]{:S(2)}) copy-start(f32[4,64,4,64]{1,0,3,2:T(4,128)} %get-tuple-element.457) | copy-start | bytes 786436
  207.1 102.0 %copy-start.11 = (s32[256]{0:T(256)S(1)}, s32[256]{0:T(256)}, u32[]{:S(2)}) copy-start(s32[256]{0:T(256)} %param.27) | copy-start | bytes 3076
  207.1 102.1 %copy-start.4 = (f32[4,64,4,64]{1,0,3,2:T(4,128)S(1)}, f32[4,64,4,64]{1,0,3,2:T(4,128)}, u32[]{:S(2)}) copy-start(f32[4,64,4,64]{1,0,3,2:T(4,128)} %get-tuple-element.452) | copy-start | bytes 786436
  207.1 102.4 %copy-start.7 = (f32[1,256,128]{1,2,0:T(8,128)S(1)}, f32[1,256,128]{1,2,0:T(8,128)}, u32[]{:S(2)}) copy-start(f32[1,256,128]{1,2,0:T(8,128)} %copy-done.6) | copy-start | bytes 393220
  207.1 105.0 %copy-start.10 = (bf16[256,128]{0,1:T(8,128)(2,1)S(1)}, bf16[256,128]{0,1:T(8,128)(2,1)}, u32[]{:S(2)}) copy-start(bf16[256,128]{0,1:T(8,128)(2,1)} %copy-done.9) | copy-start | bytes 196612
  247.7 65.1 %copy-start.15 = (bf16[256,256]{1,0:T(8,128)(2,1)S(1)}, bf16[256,256]{1,0:T(8,128)(2,1)}, u32[]{:S(2)}) copy-start(bf16[256,256]{1,0:T(8,128)(2,1)} %param.25) | copy-start | bytes 393220
  247.7 65.1 %copy-start.16 = (f32[256]{0:T(256)S(1)}, f32[256]{0:T(256)}, u32[]{:S(2)}) copy-start(f32[256]{0:T(256)} %param.28) | copy-start | bytes 3076
  309.1 5.9 %copy-start.12 = (f32[2,2048]{1,0:T(2,128)S(1)}, f32[2,2048]{1,0:T(2,128)}, u32[]{:S(2)}) copy-start(f32[2,2048]{1,0:T(2,128)} %param.31) | copy-start | bytes 49156
  309.1 5.9 %copy-start.13 = (f32[2,2048]{1,0:T(2,128)S(1)}, f32[2,2048]{1,0:T(2,128)}, u32[]{:S(2)}) copy-start(f32[2,2048]{1,0:T(2,128)} %param.32) | copy-start | bytes 49156
  309.1 28.4 %copy-start.1 = (bf16[256,512]{1,0:T(8,128)(2,1)S(1)}, bf16[256,512]{1,0:T(8,128)(2,1)}, u32[]{:S(2)}) copy-start(bf16[256,512]{1,0:T(8,128)(2,1)} %param.30) | copy-start | bytes 786436
  314.4 63.6 %all-gather.16.cloned.1.call-start = ((), (), s32[]{:S(2)}) async-start(), calls=%async_computation.7 | async-start | bytes 3932160 | tf_op jit(solution)/shard_map/all_gather | solution.py:153
  314.9 79.7 %all-gather.10.cloned.1.call-start = ((), (), s32[]{:S(2)}) async-start(), calls=%async_computation.3 | async-start | bytes 1310720 | tf_op jit(solution)/shard_map/all_gather | solution.py:172
  346.6 112.8 %all-gather.12.cloned.1.call-start = ((), (), s32[]{:S(2)}) async-start(), calls=%async_computation.4 | async-start | bytes 3932160 | tf_op jit(solution)/shard_map/all_gather | solution.py:151
  347.2 175.8 %all-gather.14.cloned.1.call-start = ((), (), s32[]{:S(2)}) async-start(), calls=%async_computation.5 | async-start | bytes 3932160 | tf_op jit(solution)/shard_map/all_gather | solution.py:152
  347.9 204.9 %reduce-scatter.5.cloned.1.call-start = ((), (), s32[]{:S(2)}) async-start(), calls=%async_computation.6 | async-start | bytes 1310720 | tf_op jit(solution)/shard_map/reduce_scatter | solution.py:176
  394.7 128.4 %copy-start.14 = (bf16[256,2048]{1,0:T(8,128)(2,1)S(1)}, bf16[256,2048]{1,0:T(8,128)(2,1)}, u32[]{:S(2)}) copy-start(bf16[256,2048]{1,0:T(8,128)(2,1)} %all-gather.10.cloned.1.call-done) | copy-start | bytes 3145732
  523.0 29.9 %copy-start.2 = (bf16[256,512]{1,0:T(8,128)(2,1)S(1)}, bf16[256,512]{1,0:T(8,128)(2,1)}, u32[]{:S(2)}) copy-start(bf16[256,512]{1,0:T(8,128)(2,1)} %reduce-scatter.3.cloned.1.call-done) | copy-start | bytes 786436
Sparse Core Ops, SparseCore 0:
  314.5 23.0 reduce-scatter.2
  529.4 23.4 reduce-scatter.4
Sparse Core Ops, SparseCore 1:
  316.4 61.5 all-gather.15
  379.4 15.2 all-gather.9
  396.1 63.3 all-gather.11
  461.0 61.9 all-gather.13
